TPU v7x, 32 devices: a whole 2x2x4 slice. The times are simulated.
32 devices in a mesh: grp: 2 (over y), ra: 4 (over z), cb: 4 (over x, core).
Axes of the slice: x: 2, y: 2, z: 4, core: 2. Of those that a mesh axis runs over, the one named last changes fastest.
Arguments:
- tokens: bfloat16 [256, 2048], P('grp', 'ra'), parts along dimension 0, may hold values from -8 to 8
- first_gain: bfloat16 [2048], P('ra'), may hold values from 0.099609375 to 1.8984375
- first_gate: bfloat16 [2048, 5632], P('ra', 'cb'), may hold values from -0.125 to 0.125
- first_up: bfloat16 [2048, 5632], P('ra', 'cb'), may hold values from -0.125 to 0.125
- first_down: bfloat16 [5632, 2048], P('cb', 'ra'), may hold values from -0.078125 to 0.078125
- second_gain: bfloat16 [2048], P('ra'), may hold values from 0.099609375 to 1.8984375
- second_gate: bfloat16 [2048, 5632], P('ra', 'cb'), may hold values from -0.125 to 0.125
- second_up: bfloat16 [2048, 5632], P('ra', 'cb'), may hold values from -0.125 to 0.125
- second_down: bfloat16 [5632, 2048], P('cb', 'ra'), may hold values from -0.078125 to 0.078125
Outputs:
- latent_out: bfloat16 [256, 2048], P('grp', 'ra'), parts along dimension 0
There are 2 independent parts, one for each index of `grp`. A program takes and returns all parts, laid end to end along the dimension named above; an argument that names none is the same for every part. Nothing has to cross between parts.
All inputs are finite; a program needn't handle non-finite values.
Results may differ from a plain program's by a relative error of at most 0.0088.
Values may be sent and summed in bfloat16 or wider, within the bound.
No kernel may reach another device: no remote copies, remote signals or barrier semaphores. Data moves between devices by JAX's collectives and lax.ppermute only.
A program may use at most 64 MiB of HBM per device.

v0:
```python
import jax
import jax.numpy as jnp
from jax import lax
from jax.sharding import PartitionSpec as P


def sublayer(x, gain, w_gate, w_up, w_down):
    xf = x.astype(jnp.float32)
    width = x.shape[1] * lax.axis_size("ra")
    rows = x.shape[0]
    squares = jnp.sum(xf * xf, axis=1)
    normed = (xf * gain.astype(jnp.float32)).astype(jnp.bfloat16)
    dims = (((0,), (1,)), ((), ()))
    gate_rows = lax.dot_general(w_gate, normed, dims, preferred_element_type=jnp.float32)
    up_rows = lax.dot_general(w_up, normed, dims, preferred_element_type=jnp.float32)
    shares = lax.psum_scatter(
        jnp.concatenate([gate_rows, up_rows], axis=1), "ra", scatter_dimension=0, tiled=True
    )
    total_sq = lax.psum(squares, "ra")
    scale = lax.rsqrt(total_sq / width + 1e-06)
    hidden_t = (
        jax.nn.silu(shares[:, :rows] * scale[None, :]) * (shares[:, rows:] * scale[None, :])
    ).astype(jnp.bfloat16)
    partial_value = lax.dot_general(
        lax.all_gather(hidden_t, "ra", axis=0, tiled=True),
        w_down,
        (((0,), (0,)), ((), ())),
        preferred_element_type=jnp.float32,
    )
    branch = lax.psum(partial_value, "cb")
    return (0.5 * xf + 0.5 * branch).astype(jnp.bfloat16)


def per_device(
    tokens,
    first_gain,
    first_gate,
    first_up,
    first_down,
    second_gain,
    second_gate,
    second_up,
    second_down,
):
    middle = sublayer(tokens, first_gain, first_gate, first_up, first_down)
    return sublayer(middle, second_gain, second_gate, second_up, second_down)


def solution(mesh):
    placed = (
        P("grp", "ra"),
        P("ra"),
        P("ra", "cb"),
        P("ra", "cb"),
        P("cb", "ra"),
        P("ra"),
        P("ra", "cb"),
        P("ra", "cb"),
        P("cb", "ra"),
    )
    return jax.shard_map(
        per_device, mesh=mesh, in_specs=placed, out_specs=P("grp", "ra"), check_vma=False
    )
```

profile of v0, /device:TPU:0, one launch (start us, length us, event | category | flops | bytes accessed | tf_op | source)
XLA Modules:
  0.0 194.4 jit_solution(9216063514448310554)
XLA Ops:
  6.5 0.8 convert_element_type.31
  7.4 0.5 copy-done
  7.9 1.3 convolution_bitcast_fusion.2
  9.2 0.4 convolution_bitcast_fusion.3
  9.6 0.1 pad_maximum_fusion
  9.7 1.6 copy.12
  11.3 0.1 fusion.1
  11.5 13.6 %psum.28 = f32[128]{0:T(128)S(1)} all-reduce(f32[128]{0:T(128)S(1)} %fusion.1), channel_id=1, replica_groups=mesh['grp'=2,'ra'=4,'cb'=4] {'ra'}, use_global_device_ids=true, to_apply=%region_2.0 | all-reduce | flops 128 | bytes 1024 | tf_op jit(solution)/shard_map/psum | solution.py:19
  25.1 22.5 %reduce-scatter.7.cloned.1.call-done = f32[352,256]{1,0:T(8,128)} async-done(((f32[1408,256]{1,0:T(8,128)}), f32[352,256]{1,0:T(8,128)}) %reduce-scatter.7.cloned.1.call-update) | async-done | bytes 360464
  47.6 1.7 fusion.14
  49.3 0.1 copy.16
  49.4 1.1 copy.17
  50.5 0.1 multiply_convert_fusion.1
  50.6 0.1 copy.10
  50.8 15.0 %all_gather.6 = bf16[1408,128]{1,0:T(8,128)(2,1)S(1)} all-gather(bf16[352,128]{1,0:T(8,128)(2,1)S(1)} %copy.10), channel_id=1, replica_groups=mesh['grp'=2,'ra'=4,'cb'=4] {'ra'}, dimensions={0}, use_global_device_ids=true | all-gather | bytes 450560 | tf_op jit(solution)/shard_map/all_gather | solution.py:25
  65.8 1.1 fusion.15
  67.0 30.7 %all-reduce.3.cloned.1.call-done = f32[128,512]{1,0:T(8,128)} async-done(((f32[128,512]{1,0:T(8,128)}), f32[128,512]{1,0:T(8,128)}) %all-reduce.3.cloned.1.call-update) | async-done | bytes 262160 | tf_op jit(solution)/shard_map/psum | solution.py:30
  97.7 1.1 fusion.5
  98.8 1.7 convolution_bitcast_fusion
  100.5 0.4 convolution_bitcast_fusion.1
  101.0 1.6 copy.14
  102.6 12.1 %psum.30 = f32[128]{0:T(128)S(1)} all-reduce(f32[128]{0:T(128)S(1)} %get-tuple-element.5), channel_id=1, replica_groups=mesh['grp'=2,'ra'=4,'cb'=4] {'ra'}, use_global_device_ids=true, to_apply=%region_6.7 | all-reduce | flops 128 | bytes 1024 | tf_op jit(solution)/shard_map/psum | solution.py:19
  114.7 21.5 %reduce-scatter.9.cloned.1.call-done = f32[352,256]{1,0:T(8,128)} async-done(((f32[1408,256]{1,0:T(8,128)}), f32[352,256]{1,0:T(8,128)}) %reduce-scatter.9.cloned.1.call-update) | async-done | bytes 360464
  136.2 1.7 fusion.13
  137.9 0.1 copy.18
  138.0 1.1 copy.19
  139.1 0.1 multiply_convert_fusion
  139.2 0.1 copy.11
  139.3 15.1 %all_gather.7 = bf16[1408,128]{1,0:T(8,128)(2,1)S(1)} all-gather(bf16[352,128]{1,0:T(8,128)(2,1)S(1)} %copy.11), channel_id=1, replica_groups=mesh['grp'=2,'ra'=4,'cb'=4] {'ra'}, dimensions={0}, use_global_device_ids=true | all-gather | bytes 450560 | tf_op jit(solution)/shard_map/all_gather | solution.py:25
  154.4 1.1 fusion.16
  155.5 30.7 %all-reduce.5.cloned.1.call-done = f32[128,512]{1,0:T(8,128)} async-done(((f32[128,512]{1,0:T(8,128)}), f32[128,512]{1,0:T(8,128)}) %all-reduce.5.cloned.1.call-update) | async-done | bytes 262160 | tf_op jit(solution)/shard_map/psum | solution.py:30
  186.2 1.6 fusion.7
  (25 shorter events, 0.3 us)
Async XLA Ops:
  6.5 1.4 copy-start
  6.5 2.7 %copy-start.1 = (bf16[128,512]{1,0:T(8,128)(2,1)S(1)}, bf16[128,512]{1,0:T(8,128)(2,1)}, u32[]{:S(2)}) copy-start(bf16[128,512]{1,0:T(8,128)(2,1)} %param.9) | copy-start | bytes 393220
  6.5 2.7 %copy-start.2 = (bf16[512,1408]{1,0:T(8,128)(2,1)S(1)}, bf16[512,1408]{1,0:T(8,128)(2,1)}, u32[]{:S(2)}) copy-start(bf16[512,1408]{1,0:T(8,128)(2,1)} %param.11) | copy-start | bytes 4325380
  6.5 41.1 %reduce-scatter.7.cloned.1.call-start = ((), (), s32[]{:S(2)}) async-start(), calls=%async_computation.4 | async-start | bytes 1802240
  11.3 54.5 %copy-start.3 = (bf16[1408,512]{1,0:T(8,128)(2,1)S(1)}, bf16[1408,512]{1,0:T(8,128)(2,1)}, u32[]{:S(2)}) copy-start(bf16[1408,512]{1,0:T(8,128)(2,1)} %param.13) | copy-start | bytes 4325380
  11.3 86.4 %all-reduce.3.cloned.1.call-start = ((), (), s32[]{:S(2)}) async-start(), calls=%async_computation.2 | async-start | bytes 524288 | tf_op jit(solution)/shard_map/psum | solution.py:30
  50.6 16.3 %copy-start.6 = (bf16[512]{0:T(512)(128)(2,1)S(1)}, bf16[512]{0:T(512)(128)(2,1)}, u32[]{:S(2)}) copy-start(bf16[512]{0:T(512)(128)(2,1)} %param.14) | copy-start | bytes 3076
  66.9 33.6 %copy-start.4 = (bf16[512,1408]{1,0:T(8,128)(2,1)S(1)}, bf16[512,1408]{1,0:T(8,128)(2,1)}, u32[]{:S(2)}) copy-start(bf16[512,1408]{1,0:T(8,128)(2,1)} %param.15) | copy-start | bytes 4325380
  66.9 69.3 %reduce-scatter.9.cloned.1.call-start = ((), (), s32[]{:S(2)}) async-start(), calls=%async_computation.5 | async-start | bytes 1802240
  102.6 51.8 %copy-start.5 = (bf16[1408,512]{1,0:T(8,128)(2,1)S(1)}, bf16[1408,512]{1,0:T(8,128)(2,1)}, u32[]{:S(2)}) copy-start(bf16[1408,512]{1,0:T(8,128)(2,1)} %param.17) | copy-start | bytes 4325380
  102.6 83.6 %all-reduce.5.cloned.1.call-start = ((), (), s32[]{:S(2)}) async-start(), calls=%async_computation.3 | async-start | bytes 524288 | tf_op jit(solution)/shard_map/psum | solution.py:30
Sparse Core Ops, SparseCore 0:
  11.4 36.1 reduce-scatter.6
  67.0 30.5 all-reduce.2
  102.7 33.4 reduce-scatter.8
  155.7 30.5 all-reduce.4
where the time goes:
time: 195 us; the launch traced here: 194 us
  waiting for transfers between devices  105 us (54%)
  blocking collectives  55.8 us (29%)
  between operations  13.3 us (7%)
  local copies, waits for them, and re-layouts  9.67 us (5%)
  matrix products  6.01 us (3%)
  other arithmetic  4.14 us (2%)
    psum x2, waiting for transfers between devices, sublayer(): branch = lax.psum(partial_value, 'cb')  61.4 us
    unnamed x6, waiting for transfers between devices  44 us
    all_gather x2, blocking collectives, sublayer(): lax.all_gather(hidden_t, 'ra', axis=0, tiled=True)  30.1 us
    psum x2, blocking collectives, sublayer(): total_sq = lax.psum(squares, 'ra')  25.7 us
    unnamed x20, local copies, waits for them, and re-layouts  6.04 us
  transfers between devices with their start and end apart: 4, of which 4 were waited for; matrix products, arithmetic and copies ran while one was open for 0% of the time, Pallas kernels for 0%

commit v1 on v0

--- a/solution.py
+++ b/solution.py
@@ -27,7 +27,8 @@
         (((0,), (0,)), ((), ())),
         preferred_element_type=jnp.float32,
     )
-    branch = lax.psum(partial_value, "cb")
+    terms = lax.all_gather(partial_value, "cb")
+    branch = jnp.sum(terms, axis=0)
     return (0.5 * xf + 0.5 * branch).astype(jnp.bfloat16)
 
 

time: 195 us -> 164 us (0.84)
  waiting for transfers between devices: 105 us -> 74.2 us
    psum x2 -> x0, waiting for transfers between devices: 61.4 us -> none  [sublayer(): branch = lax.psum(partial_value, 'cb')]
    all_gather x0 -> x2, waiting for transfers between devices: none -> 30.2 us  [sublayer(): terms = lax.all_gather(partial_value, 'cb')]
    reduce_sum x0 -> x2, other arithmetic: none -> 2.65 us  [sublayer(): branch = jnp.sum(terms, axis=0)]
    unnamed x20 -> x22, local copies, waits for them, and re-layouts: 6.04 us -> 6.87 us
where the time goes in v1:
time: 164 us; the launch traced here: 163 us
  waiting for transfers between devices  74.2 us (45%)
  blocking collectives  55.8 us (34%)
  between operations  13.3 us (8%)
  local copies, waits for them, and re-layouts  10.5 us (6%)
  other arithmetic  4.9 us (3%)
  matrix products  4.68 us (3%)
    unnamed x6, waiting for transfers between devices  44 us
    all_gather x2, waiting for transfers between devices, sublayer(): terms = lax.all_gather(partial_value, 'cb')  30.2 us
    all_gather x2, blocking collectives, sublayer(): lax.all_gather(hidden_t, 'ra', axis=0, tiled=True)  30.1 us
    psum x2, blocking collectives, sublayer(): total_sq = lax.psum(squares, 'ra')  25.7 us
    unnamed x22, local copies, waits for them, and re-layouts  6.87 us
    slice x2, local copies, waits for them, and re-layouts, sublayer(): shares[:, :rows] * scale[None, :]  3.39 us
  transfers between devices with their start and end apart: 4, of which 4 were waited for; matrix products, arithmetic and copies ran while one was open for 0% of the time, Pallas kernels for 0%

profile of v1, /device:TPU:0, one launch (start us, length us, event | category | flops | bytes accessed | tf_op | source)
XLA Modules:
  0.0 163.5 jit_solution(15558211449647257783)
XLA Ops:
  6.5 0.8 convert_element_type.31
  7.4 0.5 copy-done
  7.9 1.3 convolution_bitcast_fusion.2
  9.2 0.4 convolution_bitcast_fusion.3
  9.7 1.6 copy.12
  11.5 13.6 %psum.14 = f32[128]{0:T(128)S(1)} all-reduce(f32[128]{0:T(128)S(1)} %fusion.1), channel_id=1, replica_groups=mesh['grp'=2,'ra'=4,'cb'=4] {'ra'}, use_global_device_ids=true, to_apply=%region_2.0 | all-reduce | flops 128 | bytes 1024 | tf_op jit(solution)/shard_map/psum | solution.py:19
  25.1 22.5 %reduce-scatter.7.cloned.1.call-done = f32[352,256]{1,0:T(8,128)} async-done(((f32[1408,256]{1,0:T(8,128)}), f32[352,256]{1,0:T(8,128)}) %reduce-scatter.7.cloned.1.call-update) | async-done | bytes 360464
  47.6 1.7 %fusion.14 = (f32[352,128]{1,0:T(8,128)S(1)}, f32[352,128]{1,0:T(8,128)}) fusion(f32[352,256]{1,0:T(8,128)} %reduce-scatter.7.cloned.1.call-done), kind=kLoop, calls=%fused_computation.25 | loop fusion | bytes 720896 | tf_op jit(solution)/shard_map/slice | solution.py:22
  49.3 0.1 copy.16
  49.4 1.1 copy.17
  50.5 0.1 multiply_convert_fusion.1
  50.6 0.1 copy.10
  50.8 15.0 %all_gather.18 = bf16[1408,128]{1,0:T(8,128)(2,1)S(1)} all-gather(bf16[352,128]{1,0:T(8,128)(2,1)S(1)} %copy.10), channel_id=1, replica_groups=mesh['grp'=2,'ra'=4,'cb'=4] {'ra'}, dimensions={0}, use_global_device_ids=true | all-gather | bytes 450560 | tf_op jit(solution)/shard_map/all_gather | solution.py:25
  65.8 1.1 fusion.15
  67.0 15.1 %all-gather.5.cloned.1.call-done = f32[512,512]{1,0:T(8,128)} async-done(((f32[128,512]{1,0:T(8,128)}), f32[512,512]{1,0:T(8,128)}) %all-gather.5.cloned.1.call-update) | async-done | bytes 1048592 | tf_op jit(solution)/shard_map/all_gather | solution.py:30
  82.1 1.3 reduce_sum.37
  83.4 0.1 fusion.5
  83.6 0.4 convolution_bitcast_fusion
  84.0 0.8 copy-done.5
  84.8 0.4 convolution_bitcast_fusion.1
  85.3 1.6 copy.14
  86.9 12.1 %psum.15 = f32[128]{0:T(128)S(1)} all-reduce(f32[128]{0:T(128)S(1)} %get-tuple-element.5), channel_id=1, replica_groups=mesh['grp'=2,'ra'=4,'cb'=4] {'ra'}, use_global_device_ids=true, to_apply=%region_6.7 | all-reduce | flops 128 | bytes 1024 | tf_op jit(solution)/shard_map/psum | solution.py:19
  99.0 21.4 %reduce-scatter.9.cloned.1.call-done = f32[352,256]{1,0:T(8,128)} async-done(((f32[1408,256]{1,0:T(8,128)}), f32[352,256]{1,0:T(8,128)}) %reduce-scatter.9.cloned.1.call-update) | async-done | bytes 360464
  120.5 1.7 %fusion.13 = (f32[352,128]{1,0:T(8,128)S(1)}, f32[352,128]{1,0:T(8,128)}) fusion(f32[352,256]{1,0:T(8,128)} %reduce-scatter.9.cloned.1.call-done), kind=kLoop, calls=%fused_computation.24 | loop fusion | bytes 720896 | tf_op jit(solution)/shard_map/slice | solution.py:22
  122.2 0.1 copy.18
  122.3 1.1 copy.19
  123.3 0.1 multiply_convert_fusion
  123.6 15.1 %all_gather.21 = bf16[1408,128]{1,0:T(8,128)(2,1)S(1)} all-gather(bf16[352,128]{1,0:T(8,128)(2,1)S(1)} %copy.11), channel_id=1, replica_groups=mesh['grp'=2,'ra'=4,'cb'=4] {'ra'}, dimensions={0}, use_global_device_ids=true | all-gather | bytes 450560 | tf_op jit(solution)/shard_map/all_gather | solution.py:25
  138.7 1.1 fusion.16
  139.9 15.1 %all-gather.7.cloned.1.call-done = f32[512,512]{1,0:T(8,128)} async-done(((f32[128,512]{1,0:T(8,128)}), f32[512,512]{1,0:T(8,128)}) %all-gather.7.cloned.1.call-update) | async-done | bytes 1048592 | tf_op jit(solution)/shard_map/all_gather | solution.py:30
  154.9 1.3 reduce_sum.39
  156.3 0.7 fusion.7
  (29 shorter events, 0.7 us)
Async XLA Ops:
  6.5 1.4 copy-start
  6.5 2.7 %copy-start.1 = (bf16[128,512]{1,0:T(8,128)(2,1)S(1)}, bf16[128,512]{1,0:T(8,128)(2,1)}, u32[]{:S(2)}) copy-start(bf16[128,512]{1,0:T(8,128)(2,1)} %param.9) | copy-start | bytes 393220
  6.5 2.7 %copy-start.2 = (bf16[512,1408]{1,0:T(8,128)(2,1)S(1)}, bf16[512,1408]{1,0:T(8,128)(2,1)}, u32[]{:S(2)}) copy-start(bf16[512,1408]{1,0:T(8,128)(2,1)} %param.11) | copy-start | bytes 4325380
  6.5 41.1 %reduce-scatter.7.cloned.1.call-start = ((), (), s32[]{:S(2)}) async-start(), calls=%async_computation.4 | async-start | bytes 1802240
  11.3 54.5 %copy-start.3 = (bf16[1408,512]{1,0:T(8,128)(2,1)S(1)}, bf16[1408,512]{1,0:T(8,128)(2,1)}, u32[]{:S(2)}) copy-start(bf16[1408,512]{1,0:T(8,128)(2,1)} %param.13) | copy-start | bytes 4325380
  11.3 70.8 %all-gather.5.cloned.1.call-start = ((), (), s32[]{:S(2)}) async-start(), calls=%async_computation.2 | async-start | bytes 1310720 | tf_op jit(solution)/shard_map/all_gather | solution.py:30
  50.6 16.4 %copy-start.7 = (bf16[512]{0:T(512)(128)(2,1)S(1)}, bf16[512]{0:T(512)(128)(2,1)}, u32[]{:S(2)}) copy-start(bf16[512]{0:T(512)(128)(2,1)} %param.14) | copy-start | bytes 3076
  66.9 16.7 %copy-start.4 = (bf16[512,1408]{1,0:T(8,128)(2,1)S(1)}, bf16[512,1408]{1,0:T(8,128)(2,1)}, u32[]{:S(2)}) copy-start(bf16[512,1408]{1,0:T(8,128)(2,1)} %param.16) | copy-start | bytes 4325380
  66.9 53.5 %reduce-scatter.9.cloned.1.call-start = ((), (), s32[]{:S(2)}) async-start(), calls=%async_computation.5 | async-start | bytes 1802240
  83.4 1.4 copy-start.5
  86.9 51.8 %copy-start.6 = (bf16[1408,512]{1,0:T(8,128)(2,1)S(1)}, bf16[1408,512]{1,0:T(8,128)(2,1)}, u32[]{:S(2)}) copy-start(bf16[1408,512]{1,0:T(8,128)(2,1)} %param.17) | copy-start | bytes 4325380
  86.9 68.1 %all-gather.7.cloned.1.call-start = ((), (), s32[]{:S(2)}) async-start(), calls=%async_computation.3 | async-start | bytes 1310720 | tf_op jit(solution)/shard_map/all_gather | solution.py:30
Sparse Core Ops, SparseCore 0:
  11.4 36.1 reduce-scatter.6
  67.1 14.9 all-gather.4
  87.0 33.4 reduce-scatter.8
  140.0 14.9 all-gather.6
